TPU v7x, 256 devices: a whole 4x4x8 slice. The times are simulated.
256 devices in a mesh: sp: 32 (over z, x), fs: 4 (over y), tp: 2 (over core).
Axes of the slice: x: 4, y: 4, z: 8, core: 2. Of those that a mesh axis runs over, the one named last changes fastest.
Arguments:
- inputs: bfloat16 [4, 4096, 2048], P('fs', 'sp'), may hold values from -6 to 6
- input_norm_gain: bfloat16 [2048], replicated, may hold values from 0.099609375 to 1.8984375
- receptance_matrix: bfloat16 [2048, 1024], P('fs', 'tp'), may hold values from -0.125 to 0.125
- key_matrix: bfloat16 [2048, 1024], P('fs', 'tp'), may hold values from -0.125 to 0.125
- value_matrix: bfloat16 [2048, 1024], P('fs', 'tp'), may hold values from -0.125 to 0.125
- pooling_input_weight: bfloat16 [2048, 1024], P('fs', 'tp'), may hold values from -0.125 to 0.125
- decay_lower_matrix: bfloat16 [2048, 128], replicated, may hold values from -0.125 to 0.125
- decay_raise_matrix: bfloat16 [2, 64, 1024], P(None, None, 'tp'), may hold values from -1 to 1
- decay_offset_bias: float32 [2, 1024], P(None, 'tp'), may hold values from -13 to -3
- removal_lower_matrix: bfloat16 [2048, 128], replicated, may hold values from -0.125 to 0.125
- removal_raise_matrix: bfloat16 [2, 64, 1024], P(None, None, 'tp'), may hold values from -1 to 1
- removal_rate_bias: float32 [2, 1024], P(None, 'tp'), may hold values from -9 to 1.5
- tempo_scale: float32 [4, 2, 16, 4096], P('fs', None, 'tp', 'sp'), may hold values from 0.3 to 3.2, as said below
- sudden_decay_extra: float32 [4, 2, 16, 4096], P('fs', None, 'tp', 'sp'), may hold values from -2.8 to 0
- head_norm_gain: bfloat16 [1024], P('tp'), may hold values from 0.099609375 to 1.8984375
- group_mixing_weight: bfloat16 [4, 256, 256], P('tp'), may hold values from -0.375 to 0.375
- attention_output_matrix: bfloat16 [2048, 1024], P('fs', 'tp'), may hold values from -0.125 to 0.125
- pooling_output_matrix: bfloat16 [2048, 1024], P('fs', 'tp'), may hold values from -0.125 to 0.125
Outputs:
- mixed_out: bfloat16 [4, 4096, 2048], P('fs', ('sp', 'tp'))
Inputs may be any that keep to these rules, and one draw needn't show every extreme that they name: `tempo_scale`: positive.
All inputs are finite; a program needn't handle non-finite values.
Results may differ from a plain program's by a relative error of at most 0.017.
Values may be sent and summed in bfloat16 or wider, within the bound.
No kernel may reach another device: no remote copies, remote signals or barrier semaphores. Data moves between devices by JAX's collectives and lax.ppermute only.
A program may use at most 128 MiB of HBM per device.

v0:
```python
import jax
import jax.numpy as jnp
from jax import lax
from jax.sharding import Mesh
from jax.sharding import PartitionSpec as P

HEAD = 64
DECAY_RANK = 64
RATE_RANK = 64
POOL_GROUPS = 4
GROUP_WIDTH = 256
SP = ("sp_0", "sp_1")
SP_TP = ("sp_0", "sp_1", "tp")
norm_eps = 1e-06
head_eps = 0.00064
unit_eps = 1e-06
span_len = 32
highest = lax.Precision.HIGHEST


def filled_with(shard, identity):
    return jax.tree.map(
        lambda a, e: jnp.broadcast_to(jnp.asarray(e, a.dtype), a.shape), shard, identity
    )


def prefix_by_axis(shard, axes, combine, identity, reverse):
    before = start = filled_with(shard, identity)
    total = shard
    for axis in reversed(axes):
        peers, here = (lax.axis_size(axis), lax.axis_index(axis))
        pieces = jax.tree.map(
            lambda part, kind: lax.all_gather(part.astype(kind), axis),
            total,
            (jnp.bfloat16, jnp.bfloat16),
        )
        inside, total = (start, start)
        for k in reversed(range(peers)) if reverse else range(peers):
            passed = k > here if reverse else k < here
            total = combine(
                total, jax.tree.map(lambda part, own: part[k].astype(own.dtype), pieces, shard)
            )
            inside = jax.tree.map(lambda new, old: jnp.where(passed, new, old), total, inside)
        before = combine(inside, before)
    return before


def with_halo(cells, sides, width):
    for axis, dim in sides:
        count = lax.axis_size(axis)
        ends = count - 1
        head = lax.slice_in_dim(cells, 0, width, axis=dim)
        tail = lax.slice_in_dim(cells, cells.shape[dim] - width, cells.shape[dim], axis=dim)
        cells = jnp.concatenate(
            [
                lax.ppermute(tail, axis, [(i, (i + 1) % count) for i in range(ends)]),
                cells,
                lax.ppermute(head, axis, [((i + 1) % count, i) for i in range(ends)]),
            ],
            axis=dim,
        )
    return cells


def contract(form, left, right):
    return jnp.einsum(form, left, right, precision=highest)


def matmul(left, right):
    return contract("...ij,...jk->...ik", left, right)


def project(left, weight):
    return jnp.dot(left, weight, preferred_element_type=jnp.float32).astype(jnp.bfloat16)


def against(row_block, weight):
    return lax.dot_general(
        row_block, weight, (((1,), (1,)), ((), ())), preferred_element_type=jnp.float32
    )


def chain_combine(earlier, later):
    return (matmul(earlier[0], later[0]), matmul(earlier[1], later[0]) + later[1])


def unit_inverse(lower):
    result = jnp.eye(lower.shape[-1], dtype=jnp.float32) - lower
    power = lower
    for level in range(4):
        power = matmul(power, power)
        result = result + matmul(result, power)
    return result


def span_terms(logarithm_decay, unit, removal, written, value, recept):
    inner = jnp.cumsum(logarithm_decay, axis=-2)
    last = inner[..., -1:, :]
    ahead = unit * jnp.exp(inner - logarithm_decay)
    shrink = jnp.exp(-inner)
    remove_scaled = removal * shrink
    write_scaled = written * shrink
    query = recept * jnp.exp(inner)
    spots = jnp.arange(span_len)
    strict = spots[:, None] > spots[None, :]
    within = spots[:, None] >= spots[None, :]
    link_remove = jnp.where(strict, contract("...tk,...sk->...ts", ahead, remove_scaled), 0.0)
    link_write = jnp.where(strict, contract("...tk,...sk->...ts", ahead, write_scaled), 0.0)
    read_remove = jnp.where(within, contract("...tk,...sk->...ts", query, remove_scaled), 0.0)
    read_write = jnp.where(within, contract("...tk,...sk->...ts", query, write_scaled), 0.0)
    inverse = unit_inverse(link_remove)
    pull_map = -matmul(inverse, ahead)
    pull_base = -matmul(inverse, matmul(link_write, value))
    tail = jnp.exp(last - inner)
    remove_tail = removal * tail
    write_tail = written * tail
    transfer = jnp.eye(unit.shape[-1], dtype=jnp.float32) * jnp.exp(last) + contract(
        "...sk,...sj->...kj", pull_map, remove_tail
    )
    carried = contract("...sv,...sk->...vk", pull_base, remove_tail) + contract(
        "...sv,...sk->...vk", value, write_tail
    )
    query_eff = query + matmul(read_remove, pull_map)
    local_read = matmul(read_remove, pull_base) + matmul(read_write, value)
    return (query_eff, local_read, transfer, carried)


def shards(
    inputs,
    input_norm_gain,
    receptance_matrix,
    key_matrix,
    value_matrix,
    pooling_input_weight,
    decay_lower_matrix,
    decay_raise_matrix,
    decay_offset_bias,
    removal_lower_matrix,
    removal_raise_matrix,
    removal_rate_bias,
    tempo_scale,
    sudden_decay_extra,
    head_norm_gain,
    group_mixing_weight,
    attention_output_matrix,
    pooling_output_matrix,
):
    recept_full, key_full, value_full, pool_full, attn_full, pool_back = (
        lax.all_gather(receptance_matrix, "fs", axis=0, tiled=True),
        lax.all_gather(key_matrix, "fs", axis=0, tiled=True),
        lax.all_gather(value_matrix, "fs", axis=0, tiled=True),
        lax.all_gather(pooling_input_weight, "fs", axis=0, tiled=True),
        lax.all_gather(attention_output_matrix, "fs", axis=0, tiled=True),
        lax.all_gather(pooling_output_matrix, "fs", axis=0, tiled=True),
    )
    row_block = inputs[0].astype(jnp.float32)
    normed = (
        row_block
        * lax.rsqrt(jnp.mean(row_block * row_block, axis=-1, keepdims=True) + norm_eps)
        * input_norm_gain.astype(jnp.float32)
    ).astype(jnp.bfloat16)
    tokens = normed.shape[0]
    heads = recept_full.shape[1] // HEAD
    blocks = tokens // span_len
    receptance = project(normed, recept_full).astype(jnp.float32).reshape(tokens, heads, HEAD)
    key_rows = project(normed, key_full).astype(jnp.float32).reshape(tokens, heads, HEAD)
    val_rows = project(normed, value_full).astype(jnp.float32).reshape(tokens, heads, HEAD)
    pool_in = project(normed, pool_full)
    decay_act = jnp.tanh(project(normed, decay_lower_matrix).astype(jnp.float32)).astype(
        jnp.bfloat16
    )
    rate_latent = project(normed, removal_lower_matrix)
    unit_keys = key_rows * lax.rsqrt(
        jnp.sum(key_rows * key_rows, axis=-1, keepdims=True) + unit_eps
    )
    decays = []
    removals = []
    writes = []
    for travel_direction in range(2):
        part = decay_act[:, travel_direction * DECAY_RANK : (travel_direction + 1) * DECAY_RANK]
        decay_pre = decay_offset_bias[travel_direction] + jnp.dot(
            part, decay_raise_matrix[travel_direction], preferred_element_type=jnp.float32
        )
        decay_velocity = jnp.exp(-jax.nn.softplus(-decay_pre) - 0.5).reshape(tokens, heads, HEAD)
        decays.append(
            -decay_velocity * tempo_scale[0, travel_direction].T[:, :, None]
            + sudden_decay_extra[0, travel_direction].T[:, :, None]
        )
        latent = rate_latent[:, travel_direction * RATE_RANK : (travel_direction + 1) * RATE_RANK]
        rate = jax.nn.sigmoid(
            removal_rate_bias[travel_direction]
            + jnp.dot(
                latent, removal_raise_matrix[travel_direction], preferred_element_type=jnp.float32
            )
        )
        rate = rate.reshape(tokens, heads, HEAD)
        removals.append(unit_keys * rate)
        writes.append(key_rows * rate)

    def both_ways(forward, backward):
        stacked = jnp.stack([forward, jnp.flip(backward, axis=0)], axis=0)
        return stacked.reshape(2, blocks, span_len, heads, HEAD).transpose(0, 3, 1, 2, 4)

    query_eff, local_read, transfer, carried = span_terms(
        both_ways(decays[0], decays[1]),
        both_ways(unit_keys, unit_keys),
        both_ways(removals[0], removals[1]),
        both_ways(writes[0], writes[1]),
        both_ways(val_rows, val_rows),
        both_ways(receptance, receptance),
    )
    prefix_map, prefix_sum = lax.associative_scan(chain_combine, (transfer, carried), axis=2)
    total_map = prefix_map[:, :, -1]
    total_sum = prefix_sum[:, :, -1]
    identity_map = jnp.broadcast_to(jnp.eye(HEAD, dtype=jnp.float32), total_map.shape[1:])
    empty = jnp.zeros(total_map.shape[1:], jnp.float32)
    ahead_in = prefix_by_axis(
        (total_map[0], total_sum[0]), SP, chain_combine, (identity_map, empty), False
    )
    behind_in = prefix_by_axis(
        (total_map[1], total_sum[1]), SP, chain_combine, (identity_map, empty), True
    )
    incoming = jnp.stack([ahead_in[1], behind_in[1]], axis=0)
    ending = matmul(incoming[:, :, None], prefix_map) + prefix_sum
    starting = jnp.concatenate([incoming[:, :, None], ending[:, :, :-1]], axis=2)
    reads = contract("...tk,...vk->...tv", query_eff, starting) + local_read
    reads = reads.transpose(0, 2, 3, 1, 4).reshape(2, tokens, heads, HEAD)
    readout = reads[0] + jnp.flip(reads[1], axis=0)
    centred = readout - jnp.mean(readout, axis=-1, keepdims=True)
    spread = jnp.mean(centred * centred, axis=-1, keepdims=True)
    attn_out = (centred * lax.rsqrt(spread + head_eps)).reshape(
        tokens, heads * HEAD
    ) * head_norm_gain.astype(jnp.float32)
    attn_out = attn_out.astype(jnp.bfloat16)
    reach = 2 ** (POOL_GROUPS - 1)
    rimmed = with_halo(pool_in, ((SP, 0),), reach).astype(jnp.float32)
    position = lax.axis_index(SP) * tokens + jnp.arange(tokens)
    length = tokens * lax.axis_size(SP)
    running = rimmed
    window_sums = []
    window_counts = []
    for level in range(POOL_GROUPS):
        shift = 2**level
        running = running[:-shift] + running[shift:]
        window_sums.append(running[reach - shift : reach - shift + tokens])
        upper = jnp.minimum(position + shift, length)
        lower = jnp.maximum(position - shift, 0)
        window_counts.append((upper - lower).astype(jnp.float32))
    window_sums = jnp.stack(window_sums, axis=0)
    window_counts = jnp.stack(window_counts, axis=0)
    pool_vals = pool_in.astype(jnp.float32)
    groups_here = pool_in.shape[1] // GROUP_WIDTH
    diffs = []
    for member in range(groups_here):
        group = lax.axis_index("tp") * groups_here + member
        chosen = lax.dynamic_index_in_dim(
            window_sums[:, :, member * GROUP_WIDTH : (member + 1) * GROUP_WIDTH],
            group,
            0,
            keepdims=False,
        )
        count = lax.dynamic_index_in_dim(window_counts, group, 0, keepdims=False)
        diffs.append(
            chosen / count[:, None]
            - pool_vals[:, member * GROUP_WIDTH : (member + 1) * GROUP_WIDTH]
        )
    pool_diff = jnp.concatenate(diffs, axis=1).astype(jnp.bfloat16)
    mixed = [
        jnp.dot(
            pool_diff[:, member * GROUP_WIDTH : (member + 1) * GROUP_WIDTH],
            group_mixing_weight[member],
            preferred_element_type=jnp.float32,
        )
        for member in range(groups_here)
    ]
    pool_out = jnp.concatenate(mixed, axis=1).astype(jnp.bfloat16)
    attn_half, pool_half = (
        lax.all_to_all(attn_out, "tp", split_axis=0, concat_axis=1, tiled=True),
        lax.all_to_all(pool_out, "tp", split_axis=0, concat_axis=1, tiled=True),
    )
    attn_whole, pool_whole = (
        lax.all_gather(attn_full, "tp", axis=1, tiled=True),
        lax.all_gather(pool_back, "tp", axis=1, tiled=True),
    )
    result = against(attn_half, attn_whole) + against(pool_half, pool_whole)
    return result.astype(jnp.bfloat16)[None]


def solution(mesh):
    split = Mesh(
        mesh.devices.reshape(8, 4, mesh.shape["fs"], mesh.shape["tp"]), ("sp_0", "sp_1", "fs", "tp")
    )
    in_specs = (
        P("fs", SP, None),
        P(),
        P("fs", "tp"),
        P("fs", "tp"),
        P("fs", "tp"),
        P("fs", "tp"),
        P(),
        P(None, None, "tp"),
        P(None, "tp"),
        P(),
        P(None, None, "tp"),
        P(None, "tp"),
        P("fs", None, "tp", SP),
        P("fs", None, "tp", SP),
        P("tp"),
        P("tp", None, None),
        P("fs", "tp"),
        P("fs", "tp"),
    )
    out_specs = P("fs", SP_TP, None)
    return jax.shard_map(
        shards, mesh=split, in_specs=in_specs, out_specs=out_specs, check_vma=False
    )
```

profile of v0, /device:TPU:7, one launch (start us, length us, event | category | flops | bytes accessed | tf_op | source)
XLA Modules:
  0.0 448.1 jit_solution(15655499817770157762)
XLA Ops:
  18.1 27.2 %all-gather.19.cloned.1.call-done = bf16[2048,512]{1,0:T(8,128)(2,1)} async-done(((bf16[512,512]{1,0:T(8,128)(2,1)}), bf16[2048,512]{1,0:T(8,128)(2,1)}) %all-gather.19.cloned.1.call-update) | async-done | bytes 2097168 | tf_op jit(solution)/shard_map/all_gather | solution.py:150
  47.6 32.9 %all-gather.21.cloned.1.call-done = bf16[2048,512]{1,0:T(8,128)(2,1)} async-done(((bf16[512,512]{1,0:T(8,128)(2,1)}), bf16[2048,512]{1,0:T(8,128)(2,1)}) %all-gather.21.cloned.1.call-update) | async-done | bytes 2097168 | tf_op jit(solution)/shard_map/all_gather | solution.py:151
  90.6 3.0 fusion.55
  93.6 3.0 convolution_select_fusion.2
  105.1 2.2 convolution_add_fusion.3
  107.3 4.0 convolution_select_fusion.1
  114.5 3.2 convolution_add_fusion.2
  122.0 4.2 fusion.46
  126.3 5.0 %multiply_add_fusion = f32[2,8,4,64,64]{4,3,2,1,0:T(8,128)S(1)} fusion(f32[2,8,4,32,64]{4,3,2,1,0:T(8,128)S(1)} %convolution_negate_fusion.1, f32[2,8,4,64]{3,2,1,0:T(4,128)S(1)} %copy-done.59, f32[64,64]{1,0:T(8,128)S(1)} %fusion.167, f32[2,8,4,32,64]{4,1,2,3,0:T(8,128)} %copy-done.15), kind=kOutput, calls=%fused_computation.8 | convolution fusion | flops 101187584 | bytes 2129920 | tf_op jit(solution)/shard_map/...sk,...sj->...kj/dot_general | solution.py:66
  133.3 4.0 convolution_add_fusion.1
  145.7 11.3 %pad.33 = f32[2,8,4,64,64]{4,3,2,1,0:T(8,128)} pad(f32[2,8,2,64,64]{4,3,2,1,0:T(8,128)S(1)} %copy-done.30, f32[]{:T(128)} %constant.27.clone.1), padding=0_0_0x0_0_0x1_0_1x0_0_0x0_0_0 | pad | bytes 1572868 | tf_op jit(solution)/shard_map/pad | solution.py:212
  157.1 11.2 %pad.32 = f32[2,8,4,64,64]{4,3,2,1,0:T(8,128)} pad(f32[2,8,2,64,64]{4,3,2,1,0:T(8,128)S(1)} %pad_maximum_fusion.1, f32[]{:T(128)} %constant.27.clone.1), padding=0_0_0x0_0_0x0_1_1x0_0_0x0_0_0 | pad | bytes 1572868 | tf_op jit(solution)/shard_map/pad | solution.py:212
  168.3 11.2 %pad.28 = f32[2,8,4,64,64]{4,3,2,1,0:T(8,128)} pad(f32[2,8,2,64,64]{4,3,2,1,0:T(8,128)S(1)} %pad_maximum_fusion, f32[]{:T(128)} %constant.27.clone.1), padding=0_0_0x0_0_0x0_1_1x0_0_0x0_0_0 | pad | bytes 1572868 | tf_op jit(solution)/shard_map/pad | solution.py:212
  179.6 16.7 %pad.29 = f32[2,8,4,64,64]{4,3,2,1,0:T(8,128)} pad(f32[2,8,2,64,64]{4,3,2,1,0:T(8,128)} %pad_add_fusion.1, f32[]{:T(128)} %constant.27.clone.1), padding=0_0_0x0_0_0x1_0_1x0_0_0x0_0_0 | pad | bytes 1572868 | tf_op jit(solution)/shard_map/pad | solution.py:212
  196.3 2.2 add_convert_fusion
  198.5 10.7 %all-gather.6 = bf16[4,8,1,64,64]{4,3,2,1,0:T(8,128)(2,1)S(1)} all-gather(bf16[1,8,1,64,64]{4,3,2,1,0:T(8,128)(2,1)S(1)} %get-tuple-element.24), channel_id=8, replica_groups=mesh['sp_0'=8,'sp_1'=4,'fs'=4,'tp'=2] {'sp_1'}, dimensions={0}, use_global_device_ids=true | all-gather | bytes 327680 | tf_op jit(solution)/shard_map/all_gather | solution.py:33
  211.1 11.9 %all-gather.4 = bf16[4,8,1,64,64]{4,3,2,1,0:T(8,128)(2,1)S(1)} all-gather(bf16[1,8,1,64,64]{4,3,2,1,0:T(8,128)(2,1)S(1)} %get-tuple-element.22), channel_id=6, replica_groups=mesh['sp_0'=8,'sp_1'=4,'fs'=4,'tp'=2] {'sp_1'}, dimensions={0}, use_global_device_ids=true | all-gather | bytes 327680 | tf_op jit(solution)/shard_map/all_gather | solution.py:33
  225.7 22.8 %all-gather.7 = bf16[64,64,64]{2,1,0:T(8,128)(2,1)S(1)} all-gather(bf16[8,64,64]{2,1,0:T(8,128)(2,1)S(1)} %get-tuple-element.46), channel_id=9, replica_groups=mesh['sp_0'=8,'sp_1'=4,'fs'=4,'tp'=2] {'sp_0'}, dimensions={0}, use_global_device_ids=true | all-gather | bytes 589824 | tf_op jit(solution)/shard_map/all_gather | solution.py:33
  249.3 22.2 %all-gather.5 = bf16[64,64,64]{2,1,0:T(8,128)(2,1)S(1)} all-gather(bf16[8,64,64]{2,1,0:T(8,128)(2,1)S(1)} %get-tuple-element.48), channel_id=7, replica_groups=mesh['sp_0'=8,'sp_1'=4,'fs'=4,'tp'=2] {'sp_0'}, dimensions={0}, use_global_device_ids=true | all-gather | bytes 589824 | tf_op jit(solution)/shard_map/all_gather | solution.py:33
  273.1 10.5 %all-gather.2 = bf16[4,8,1,64,64]{4,3,2,1,0:T(8,128)(2,1)S(1)} all-gather(bf16[1,8,1,64,64]{4,3,2,1,0:T(8,128)(2,1)S(1)} %get-tuple-element.23), channel_id=4, replica_groups=mesh['sp_0'=8,'sp_1'=4,'fs'=4,'tp'=2] {'sp_1'}, dimensions={0}, use_global_device_ids=true | all-gather | bytes 327680 | tf_op jit(solution)/shard_map/all_gather | solution.py:33
  283.6 10.3 %all-gather = bf16[4,8,1,64,64]{4,3,2,1,0:T(8,128)(2,1)S(1)} all-gather(bf16[1,8,1,64,64]{4,3,2,1,0:T(8,128)(2,1)S(1)} %get-tuple-element.21), channel_id=2, replica_groups=mesh['sp_0'=8,'sp_1'=4,'fs'=4,'tp'=2] {'sp_1'}, dimensions={0}, use_global_device_ids=true | all-gather | bytes 327680 | tf_op jit(solution)/shard_map/all_gather | solution.py:33
  295.9 20.4 %all-gather.3 = bf16[64,64,64]{2,1,0:T(8,128)(2,1)S(1)} all-gather(bf16[8,64,64]{2,1,0:T(8,128)(2,1)S(1)} %get-tuple-element.50), channel_id=5, replica_groups=mesh['sp_0'=8,'sp_1'=4,'fs'=4,'tp'=2] {'sp_0'}, dimensions={0}, use_global_device_ids=true | all-gather | bytes 589824 | tf_op jit(solution)/shard_map/all_gather | solution.py:33
  317.2 21.5 %all-gather.1 = bf16[64,64,64]{2,1,0:T(8,128)(2,1)S(1)} all-gather(bf16[8,64,64]{2,1,0:T(8,128)(2,1)S(1)} %get-tuple-element.52), channel_id=3, replica_groups=mesh['sp_0'=8,'sp_1'=4,'fs'=4,'tp'=2] {'sp_0'}, dimensions={0}, use_global_device_ids=true | all-gather | bytes 589824 | tf_op jit(solution)/shard_map/all_gather | solution.py:33
  345.2 3.0 fusion.30
  363.4 3.1 convolution_select_fusion.3
  367.7 3.1 convolution_select_fusion
  376.6 3.4 fusion.9
  386.4 5.5 %collective-permute-start = (bf16[8,512]{1,0:T(8,128)(2,1)S(1)}, bf16[8,512]{1,0:T(8,128)(2,1)S(1)}, u32[]{:S(2)}, u32[]{:S(2)}) collective-permute-start(bf16[8,512]{1,0:T(8,128)(2,1)S(1)} %get-tuple-element.34), channel_id=1, source_target_pairs={{0,8},{8,16},{16,24},{24,32},{32,40},{40,48},{48,56},{56,64},{64,7... | collective-permute-start | bytes 24584 | tf_op jit(solution)/shard_map/ppermute | solution.py:56
  391.9 35.5 %all_to_all.32 = bf16[2,64,512]{2,1,0:T(8,128)(2,1)S(1)} all-to-all(bf16[2,64,512]{2,1,0:T(8,128)(2,1)S(1)} %multiply_convert_fusion), channel_id=1, replica_groups=mesh['sp_0'=8,'sp_1'=4,'fs'=4,'tp'=2] {'tp'}, dimensions={0} | all-to-all | bytes 262144 | tf_op jit(solution)/shard_map/all_to_all | solution.py:278
  429.2 3.9 all_to_all.33
  433.1 3.6 fusion.222
  436.7 4.3 fusion.1
  (338 shorter events, 95.7 us)
Async XLA Ops:
  6.5 5.0 %copy-start = (bf16[2048,128]{1,0:T(8,128)(2,1)S(1)}, bf16[2048,128]{1,0:T(8,128)(2,1)}, u32[]{:S(2)}) copy-start(bf16[2048,128]{1,0:T(8,128)(2,1)} %param.24) | copy-start | bytes 1572868
  6.5 4.7 %copy-start.68 = (f32[2,512]{1,0:T(2,128)S(1)}, f32[2,512]{1,0:T(2,128)}, u32[]{:S(2)}) copy-start(f32[2,512]{1,0:T(2,128)} %param.26) | copy-start | bytes 12292
  6.5 4.7 %copy-start.67 = (bf16[2048]{0:T(1024)(128)(2,1)S(1)}, bf16[2048]{0:T(1024)(128)(2,1)}, u32[]{:S(2)}) copy-start(bf16[2048]{0:T(1024)(128)(2,1)} %param.19) | copy-start | bytes 12292
  6.5 4.7 %copy-start.5 = (bf16[1,128,2048]{2,1,0:T(8,128)(2,1)S(1)}, bf16[1,128,2048]{2,1,0:T(8,128)(2,1)}, u32[]{:S(2)}) copy-start(bf16[1,128,2048]{2,1,0:T(8,128)(2,1)} %param.18) | copy-start | bytes 1572868
  6.5 38.7 %all-gather.19.cloned.1.call-start = ((), (), s32[]{:S(2)}) async-start(), calls=%async_computation.3 | async-start | bytes 2621440 | tf_op jit(solution)/shard_map/all_gather | solution.py:150
  7.3 73.2 %all-gather.21.cloned.1.call-start = ((), (), s32[]{:S(2)}) async-start(), calls=%async_computation.4 | async-start | bytes 2621440 | tf_op jit(solution)/shard_map/all_gather | solution.py:151
  8.0 337.1 %all-gather.17.cloned.1.call-start = ((), (), s32[]{:S(2)}) async-start(), calls=%async_computation.2 | async-start | bytes 2621440 | tf_op jit(solution)/shard_map/all_gather | solution.py:149
  8.8 339.4 %all-gather.23.cloned.1.call-start = ((), (), s32[]{:S(2)}) async-start(), calls=%async_computation.5 | async-start | bytes 2621440 | tf_op jit(solution)/shard_map/all_gather | solution.py:153
  9.3 372.0 %all-gather.29.cloned.1.call-start = ((), (), s32[]{:S(2)}) async-start(), calls=%async_computation.8 | async-start | bytes 2621440 | tf_op jit(solution)/shard_map/all_gather | solution.py:154
  10.0 372.0 %all-gather.27.cloned.1.call-start = ((), (), s32[]{:S(2)}) async-start(), calls=%async_computation.7 | async-start | bytes 2621440 | tf_op jit(solution)/shard_map/all_gather | solution.py:152
  10.5 422.6 %all-gather.25.cloned.1.call-start = ((), (), s32[]{:S(2)}) async-start(), calls=%async_computation.6 | async-start | bytes 6291456 | tf_op jit(solution)/shard_map/all_gather | solution.py:282
  11.5 69.0 %copy-start.62 = (f32[128]{0:T(128)}, f32[128]{0:T(128)S(1)}, u32[]{:S(2)}) copy-start(f32[128]{0:T(128)S(1)} %add_rsqrt_fusion.2) | copy-start | bytes 1540
  93.6 13.7 %copy-start.7 = (f32[2,8,4,32,64]{4,1,2,3,0:T(8,128)}, f32[2,8,4,32,64]{4,1,2,3,0:T(8,128)S(1)}, u32[]{:S(2)}) copy-start(f32[2,8,4,32,64]{4,1,2,3,0:T(8,128)S(1)} %get-tuple-element.12) | copy-start | bytes 1572868
  93.6 28.4 %copy-start.15 = (f32[2,8,4,32,64]{4,1,2,3,0:T(8,128)}, f32[2,8,4,32,64]{4,1,2,3,0:T(8,128)S(1)}, u32[]{:S(2)}) copy-start(f32[2,8,4,32,64]{4,1,2,3,0:T(8,128)S(1)} %get-tuple-element.16) | copy-start | bytes 1572868
  114.5 17.9 %copy-start.22 = (f32[1,4,32,8,64]{4,2,1,3,0:T(8,128)}, f32[1,4,32,8,64]{4,2,1,3,0:T(8,128)S(1)}, u32[]{:S(2)}) copy-start(f32[1,4,32,8,64]{4,2,1,3,0:T(8,128)S(1)} %copy.129) | copy-start | bytes 786436
  119.6 6.7 %copy-start.11 = (f32[2,8,4,32,64]{4,3,2,1,0:T(8,128)}, f32[2,8,4,32,64]{4,3,2,1,0:T(8,128)S(1)}, u32[]{:S(2)}) copy-start(f32[2,8,4,32,64]{4,3,2,1,0:T(8,128)S(1)} %convolution_negate_fusion.1) | copy-start | bytes 1572868
  131.3 11.3 %copy-start.2 = (f32[2,8,4,64,64]{4,3,2,1,0:T(8,128)}, f32[2,8,4,64,64]{4,3,2,1,0:T(8,128)S(1)}, u32[]{:S(2)}) copy-start(f32[2,8,4,64,64]{4,3,2,1,0:T(8,128)S(1)} %multiply_add_fusion) | copy-start | bytes 3145732
  145.6 11.3 %slice-start.1 = ((f32[2,8,4,64,64]{4,3,2,1,0:T(8,128)}), f32[2,8,1,64,64]{4,3,2,1,0:T(8,128)S(1)}, s32[]{:S(2)}) async-start(f32[2,8,4,64,64]{4,3,2,1,0:T(8,128)} %copy-done.16), calls=%async_computation.11 | async-start | bytes 1048576 | tf_op jit(solution)/shard_map/slice | solution.py:212
  145.7 11.3 %copy-start.53 = (f32[2,8,1,64,64]{4,3,2,1,0:T(8,128)S(1)}, f32[2,8,1,64,64]{4,3,2,1,0:T(8,128)}, u32[]{:S(2)}) copy-start(f32[2,8,1,64,64]{4,3,2,1,0:T(8,128)} %fusion.13) | copy-start | bytes 786436
  157.0 11.2 %slice-start = ((f32[2,8,4,64,64]{4,3,2,1,0:T(8,128)}), f32[2,8,1,64,64]{4,3,2,1,0:T(8,128)S(1)}, s32[]{:S(2)}) async-start(f32[2,8,4,64,64]{4,3,2,1,0:T(8,128)} %copy-done.2), calls=%async_computation.10 | async-start | bytes 1048576 | tf_op jit(solution)/shard_map/slice | solution.py:212
  157.0 11.2 %copy-start.54 = (f32[2,8,1,64,64]{4,3,2,1,0:T(8,128)S(1)}, f32[2,8,1,64,64]{4,3,2,1,0:T(8,128)}, u32[]{:S(2)}) copy-start(f32[2,8,1,64,64]{4,3,2,1,0:T(8,128)} %convolution_bitcast_fusion.3) | copy-start | bytes 786436
  179.6 16.7 %copy-start.3 = (f32[2,8,4,64,64]{4,3,2,1,0:T(8,128)S(1)}, f32[2,8,4,64,64]{4,3,2,1,0:T(8,128)}, u32[]{:S(2)}) copy-start(f32[2,8,4,64,64]{4,3,2,1,0:T(8,128)} %pad.33) | copy-start | bytes 3145732
  196.3 12.9 %copy-start.18 = (f32[2,8,4,64,64]{4,3,2,1,0:T(8,128)S(1)}, f32[2,8,4,64,64]{4,3,2,1,0:T(8,128)}, u32[]{:S(2)}) copy-start(f32[2,8,4,64,64]{4,3,2,1,0:T(8,128)} %pad.28) | copy-start | bytes 3145732
  196.3 12.9 %copy-start.19 = (f32[2,8,4,64,64]{4,3,2,1,0:T(8,128)S(1)}, f32[2,8,4,64,64]{4,3,2,1,0:T(8,128)}, u32[]{:S(2)}) copy-start(f32[2,8,4,64,64]{4,3,2,1,0:T(8,128)} %pad.29) | copy-start | bytes 3145732
  224.5 24.6 %copy-start.33 = (f32[8,64,64]{2,1,0:T(8,128)}, f32[8,64,64]{2,1,0:T(8,128)S(1)}, u32[]{:S(2)}) copy-start(f32[8,64,64]{2,1,0:T(8,128)S(1)} %convolution_add_fusion.19) | copy-start | bytes 393220
  224.8 24.6 %copy-start.34 = (f32[8,64,64]{2,1,0:T(8,128)}, f32[8,64,64]{2,1,0:T(8,128)S(1)}, u32[]{:S(2)}) copy-start(f32[8,64,64]{2,1,0:T(8,128)S(1)} %convolution_add_fusion.18) | copy-start | bytes 393220
  294.4 22.3 %copy-start.45 = (f32[8,64,64]{2,1,0:T(8,128)}, f32[8,64,64]{2,1,0:T(8,128)S(1)}, u32[]{:S(2)}) copy-start(f32[8,64,64]{2,1,0:T(8,128)S(1)} %convolution_add_fusion.33) | copy-start | bytes 393220
  316.4 24.8 %copy-start.26 = (bf16[64,64,64]{2,1,0:T(8,128)(2,1)}, bf16[64,64,64]{2,1,0:T(8,128)(2,1)S(1)}, u32[]{:S(2)}) copy-start(bf16[64,64,64]{2,1,0:T(8,128)(2,1)S(1)} %all-gather.3) | copy-start | bytes 1572868
  348.2 88.5 %all-gather.31.cloned.1.call-start = ((), (), s32[]{:S(2)}) async-start(), calls=%async_computation.9 | async-start | bytes 6291456 | tf_op jit(solution)/shard_map/all_gather | solution.py:283
  381.8 10.1 %copy-start.64 = (f32[512]{0:T(512)S(1)}, f32[512]{0:T(512)}, u32[]{:S(2)}) copy-start(f32[512]{0:T(512)} %convert_element_type.431) | copy-start | bytes 6148
  384.5 43.0 %collective-permute-start.1 = (bf16[8,512]{1,0:T(8,128)(2,1)S(1)}, bf16[8,512]{1,0:T(8,128)(2,1)S(1)}, u32[]{:S(2)}, u32[]{:S(2)}) collective-permute-start(bf16[8,512]{1,0:T(8,128)(2,1)S(1)} %get-tuple-element.35), channel_id=1, source_target_pairs={{8,0},{16,8},{24,16},{32,24},{40,32},{48,40},{56,48},{64,56},{72,6... | collective-permute-start | bytes 24584 | tf_op jit(solution)/shard_map/ppermute | solution.py:58
  386.4 41.1 %collective-permute-start = (bf16[8,512]{1,0:T(8,128)(2,1)S(1)}, bf16[8,512]{1,0:T(8,128)(2,1)S(1)}, u32[]{:S(2)}, u32[]{:S(2)}) collective-permute-start(bf16[8,512]{1,0:T(8,128)(2,1)S(1)} %get-tuple-element.34), channel_id=1, source_target_pairs={{0,8},{8,16},{16,24},{24,32},{32,40},{40,48},{48,56},{56,64},{64,7... | collective-permute-start | bytes 24584 | tf_op jit(solution)/shard_map/ppermute | solution.py:56
  (56 other events, 120.3 us)
Sparse Core Ops, SparseCore 0:
  9.2 36.0 all-gather.18
  47.1 33.3 all-gather.20
  82.3 33.3 all-gather.16
  117.4 33.3 all-gather.22
  152.5 33.3 all-gather.28
  187.5 33.3 all-gather.26
  348.3 47.0 all-gather.24
  397.2 31.7 all-gather.30
where the time goes:
time: 454 us; the launch traced here: 448 us
  blocking collectives  170 us (37%)
  matrix products  97.3 us (21%)
  local copies, waits for them, and re-layouts  78.8 us (17%)
  waiting for transfers between devices  63.8 us (14%)
  between operations  15.5 us (3%)
  other arithmetic  15 us (3%)
  starting transfers between devices  8.1 us (2%)
    all_gather x8, blocking collectives, prefix_by_axis(): lax.all_gather(part.astype(kind), axis)  130 us
    dot_general x67, matrix products, contract(): return jnp.einsum(form, left, right, precision=highest)  77.8 us
    pad x4, local copies, waits for them, and re-layouts, shards(): lax.associative_scan(chain_combine, (transfer, carried), axis=2)  50.4 us
    all_to_all x1, blocking collectives, shards(): lax.all_to_all(attn_out, 'tp', split_axis=0, concat_axis=1, tiled=True)  35.5 us
    all_gather x1, waiting for transfers between devices, shards(): lax.all_gather(value_matrix, 'fs', axis=0, tiled=True)  32.9 us
    all_gather x1, waiting for transfers between devices, shards(): lax.all_gather(key_matrix, 'fs', axis=0, tiled=True)  27.2 us
    dot_general x6, matrix products, project(): jnp.dot(left, weight, preferred_element_type=jnp.float32)  10 us
    rev x12, local copies, waits for them, and re-layouts, both_ways(): stacked = jnp.stack([forward, jnp.flip(backward, axis=0)], axis=0)  9.63 us
  transfers between devices with their start and end apart: 10, of which 2 were waited for; matrix products, arithmetic and copies ran while one was open for 40% of the time, Pallas kernels for 0%

commit v1 on v0

--- a/solution.py
+++ b/solution.py
@@ -16,6 +16,13 @@
 unit_eps = 1e-06
 span_len = 32
 highest = lax.Precision.HIGHEST
+
+
+def apply_the_positions(in_array):
+    degree = lax.axis_size("fs")
+    r1 = jnp.tile(in_array, [degree if h == 0 else 1 for h in range(in_array.ndim)])
+    mixed_arr = lax.all_to_all(r1, "fs", split_axis=0, concat_axis=0, tiled=True)
+    return mixed_arr
 
 
 def filled_with(shard, identity):
@@ -148,7 +155,7 @@
     recept_full, key_full, value_full, pool_full, attn_full, pool_back = (
         lax.all_gather(receptance_matrix, "fs", axis=0, tiled=True),
         lax.all_gather(key_matrix, "fs", axis=0, tiled=True),
-        lax.all_gather(value_matrix, "fs", axis=0, tiled=True),
+        apply_the_positions(value_matrix),
         lax.all_gather(pooling_input_weight, "fs", axis=0, tiled=True),
         lax.all_gather(attention_output_matrix, "fs", axis=0, tiled=True),
         lax.all_gather(pooling_output_matrix, "fs", axis=0, tiled=True),

time: 454 us -> 429 us (0.945)
  waiting for transfers between devices: 63.8 us -> 32.8 us
  matrix products: 97.3 us -> 90.9 us
  blocking collectives: 170 us -> 175 us
    all_gather x1 -> x0, waiting for transfers between devices: 32.9 us -> none  [shards(): lax.all_gather(value_matrix, 'fs', axis=0, tiled=True)]
    all_to_all x0 -> x1, waiting for transfers between devices: none -> 28.8 us  [apply_the_positions(): lax.all_to_all(r1, 'fs', split_axis=0, concat_axis=0, tiled=True)]
    all_gather x1, waiting for transfers between devices: 27.2 us -> 0.71 us  [shards(): lax.all_gather(key_matrix, 'fs', axis=0, tiled=True)]
    dot_general x67, matrix products: 77.8 us -> 71.4 us  [contract(): return jnp.einsum(form, left, right, precision=highest)]
    all_to_all x0 -> x1, starting transfers between devices: none -> 4.59 us  [apply_the_positions(): lax.all_to_all(r1, 'fs', split_axis=0, concat_axis=0, tiled=True)]
  transfers between devices with their start and end apart: 10 -> 10, of which waited for: 2 -> 2; matrix products, arithmetic and copies ran while one was open for 40% -> 42% of each run, Pallas kernels for 0% -> 0%
where the time goes in v1:
time: 429 us; the launch traced here: 423 us
  blocking collectives  175 us (41%)
  matrix products  90.9 us (21%)
  local copies, waits for them, and re-layouts  81.4 us (19%)
  waiting for transfers between devices  32.8 us (8%)
  between operations  15.6 us (4%)
  other arithmetic  15.1 us (4%)
  starting transfers between devices  12.6 us (3%)
    all_gather x8, blocking collectives, prefix_by_axis(): lax.all_gather(part.astype(kind), axis)  131 us
    dot_general x67, matrix products, contract(): return jnp.einsum(form, left, right, precision=highest)  71.4 us
    pad x4, local copies, waits for them, and re-layouts, shards(): lax.associative_scan(chain_combine, (transfer, carried), axis=2)  50.4 us
    all_to_all x1, blocking collectives, shards(): lax.all_to_all(attn_out, 'tp', split_axis=0, concat_axis=1, tiled=True)  39.9 us
    all_to_all x1, waiting for transfers between devices, apply_the_positions(): lax.all_to_all(r1, 'fs', split_axis=0, concat_axis=0, tiled=True)  28.8 us
    rev x12, local copies, waits for them, and re-layouts, both_ways(): stacked = jnp.stack([forward, jnp.flip(backward, axis=0)], axis=0)  10.5 us
    dot_general x6, matrix products, project(): jnp.dot(left, weight, preferred_element_type=jnp.float32)  10 us
  transfers between devices with their start and end apart: 10, of which 2 were waited for; matrix products, arithmetic and copies ran while one was open for 42% of the time, Pallas kernels for 0%

profile of v1, /device:TPU:7, one launch (start us, length us, event | category | flops | bytes accessed | tf_op | source)
XLA Modules:
  0.0 423.5 jit_solution(6375265814943166524)
XLA Ops:
  10.9 4.6 %all-to-all-start = ((bf16[4,512,512]{2,1,0:T(8,128)(2,1)}), bf16[4,512,512]{2,1,0:T(8,128)(2,1)}, u32[]{:S(2)}, u32[]{:S(2)}) async-start(bf16[4,512,512]{2,1,0:T(8,128)(2,1)} %tile.2), calls=%async_computation | async-start | bytes 4194304 | tf_op jit(solution)/shard_map/all_to_all | solution.py:24
  24.8 28.8 %all-to-all-done = bf16[4,512,512]{2,1,0:T(8,128)(2,1)} async-done(((bf16[4,512,512]{2,1,0:T(8,128)(2,1)}), bf16[4,512,512]{2,1,0:T(8,128)(2,1)}, u32[]{:S(2)}, u32[]{:S(2)}) %all-to-all-start) | async-done | bytes 2097184 | tf_op jit(solution)/shard_map/all_to_all | solution.py:24
  53.6 2.1 fusion.30
  73.2 3.0 convolution_select_fusion.2
  84.9 3.0 convolution_select_fusion.1
  93.3 4.2 fusion.50
  97.5 3.7 multiply_add_fusion
  103.2 4.0 convolution_add_fusion.1
  115.6 11.3 %pad.33 = f32[2,8,4,64,64]{4,3,2,1,0:T(8,128)} pad(f32[2,8,2,64,64]{4,3,2,1,0:T(8,128)S(1)} %copy-done.29, f32[]{:T(128)} %constant.27.clone.1), padding=0_0_0x0_0_0x1_0_1x0_0_0x0_0_0 | pad | bytes 1572868 | tf_op jit(solution)/shard_map/pad | solution.py:219
  127.0 11.2 %pad.32 = f32[2,8,4,64,64]{4,3,2,1,0:T(8,128)} pad(f32[2,8,2,64,64]{4,3,2,1,0:T(8,128)S(1)} %pad_maximum_fusion.1, f32[]{:T(128)} %constant.27.clone.1), padding=0_0_0x0_0_0x0_1_1x0_0_0x0_0_0 | pad | bytes 1572868 | tf_op jit(solution)/shard_map/pad | solution.py:219
  138.3 11.2 %pad.28 = f32[2,8,4,64,64]{4,3,2,1,0:T(8,128)} pad(f32[2,8,2,64,64]{4,3,2,1,0:T(8,128)S(1)} %pad_maximum_fusion, f32[]{:T(128)} %constant.27.clone.1), padding=0_0_0x0_0_0x0_1_1x0_0_0x0_0_0 | pad | bytes 1572868 | tf_op jit(solution)/shard_map/pad | solution.py:219
  149.6 16.7 %pad.29 = f32[2,8,4,64,64]{4,3,2,1,0:T(8,128)} pad(f32[2,8,2,64,64]{4,3,2,1,0:T(8,128)} %pad_add_fusion.1, f32[]{:T(128)} %constant.27.clone.1), padding=0_0_0x0_0_0x1_0_1x0_0_0x0_0_0 | pad | bytes 1572868 | tf_op jit(solution)/shard_map/pad | solution.py:219
  166.3 2.2 add_convert_fusion
  168.5 9.9 %all-gather.6 = bf16[4,8,1,64,64]{4,3,2,1,0:T(8,128)(2,1)S(1)} all-gather(bf16[1,8,1,64,64]{4,3,2,1,0:T(8,128)(2,1)S(1)} %get-tuple-element.24), channel_id=8, replica_groups=mesh['sp_0'=8,'sp_1'=4,'fs'=4,'tp'=2] {'sp_1'}, dimensions={0}, use_global_device_ids=true | all-gather | bytes 327680 | tf_op jit(solution)/shard_map/all_gather | solution.py:40
  180.3 11.1 %all-gather.4 = bf16[4,8,1,64,64]{4,3,2,1,0:T(8,128)(2,1)S(1)} all-gather(bf16[1,8,1,64,64]{4,3,2,1,0:T(8,128)(2,1)S(1)} %get-tuple-element.22), channel_id=6, replica_groups=mesh['sp_0'=8,'sp_1'=4,'fs'=4,'tp'=2] {'sp_1'}, dimensions={0}, use_global_device_ids=true | all-gather | bytes 327680 | tf_op jit(solution)/shard_map/all_gather | solution.py:40
  194.2 26.6 %all-gather.7 = bf16[64,64,64]{2,1,0:T(8,128)(2,1)S(1)} all-gather(bf16[8,64,64]{2,1,0:T(8,128)(2,1)S(1)} %get-tuple-element.46), channel_id=9, replica_groups=mesh['sp_0'=8,'sp_1'=4,'fs'=4,'tp'=2] {'sp_0'}, dimensions={0}, use_global_device_ids=true | all-gather | bytes 589824 | tf_op jit(solution)/shard_map/all_gather | solution.py:40
  221.6 21.2 %all-gather.5 = bf16[64,64,64]{2,1,0:T(8,128)(2,1)S(1)} all-gather(bf16[8,64,64]{2,1,0:T(8,128)(2,1)S(1)} %get-tuple-element.48), channel_id=7, replica_groups=mesh['sp_0'=8,'sp_1'=4,'fs'=4,'tp'=2] {'sp_0'}, dimensions={0}, use_global_device_ids=true | all-gather | bytes 589824 | tf_op jit(solution)/shard_map/all_gather | solution.py:40
  244.4 10.5 %all-gather.2 = bf16[4,8,1,64,64]{4,3,2,1,0:T(8,128)(2,1)S(1)} all-gather(bf16[1,8,1,64,64]{4,3,2,1,0:T(8,128)(2,1)S(1)} %get-tuple-element.23), channel_id=4, replica_groups=mesh['sp_0'=8,'sp_1'=4,'fs'=4,'tp'=2] {'sp_1'}, dimensions={0}, use_global_device_ids=true | all-gather | bytes 327680 | tf_op jit(solution)/shard_map/all_gather | solution.py:40
  254.9 9.9 %all-gather = bf16[4,8,1,64,64]{4,3,2,1,0:T(8,128)(2,1)S(1)} all-gather(bf16[1,8,1,64,64]{4,3,2,1,0:T(8,128)(2,1)S(1)} %get-tuple-element.21), channel_id=2, replica_groups=mesh['sp_0'=8,'sp_1'=4,'fs'=4,'tp'=2] {'sp_1'}, dimensions={0}, use_global_device_ids=true | all-gather | bytes 327680 | tf_op jit(solution)/shard_map/all_gather | solution.py:40
  266.8 20.6 %all-gather.3 = bf16[64,64,64]{2,1,0:T(8,128)(2,1)S(1)} all-gather(bf16[8,64,64]{2,1,0:T(8,128)(2,1)S(1)} %get-tuple-element.50), channel_id=5, replica_groups=mesh['sp_0'=8,'sp_1'=4,'fs'=4,'tp'=2] {'sp_0'}, dimensions={0}, use_global_device_ids=true | all-gather | bytes 589824 | tf_op jit(solution)/shard_map/all_gather | solution.py:40
  288.3 21.5 %all-gather.1 = bf16[64,64,64]{2,1,0:T(8,128)(2,1)S(1)} all-gather(bf16[8,64,64]{2,1,0:T(8,128)(2,1)S(1)} %get-tuple-element.52), channel_id=3, replica_groups=mesh['sp_0'=8,'sp_1'=4,'fs'=4,'tp'=2] {'sp_0'}, dimensions={0}, use_global_device_ids=true | all-gather | bytes 589824 | tf_op jit(solution)/shard_map/all_gather | solution.py:40
  316.2 3.0 fusion.32
  319.6 2.1 fusion.16
  334.4 3.1 convolution_select_fusion.3
  338.7 3.1 convolution_select_fusion
  347.6 3.4 fusion.9
  353.4 2.1 fusion.221
  357.4 5.5 %collective-permute-start = (bf16[8,512]{1,0:T(8,128)(2,1)S(1)}, bf16[8,512]{1,0:T(8,128)(2,1)S(1)}, u32[]{:S(2)}, u32[]{:S(2)}) collective-permute-start(bf16[8,512]{1,0:T(8,128)(2,1)S(1)} %get-tuple-element.34), channel_id=1, source_target_pairs={{0,8},{8,16},{16,24},{24,32},{32,40},{40,48},{48,56},{56,64},{64,7... | collective-permute-start | bytes 24584 | tf_op jit(solution)/shard_map/ppermute | solution.py:63
  363.0 39.9 %all_to_all.41 = bf16[2,64,512]{2,1,0:T(8,128)(2,1)S(1)} all-to-all(bf16[2,64,512]{2,1,0:T(8,128)(2,1)S(1)} %multiply_convert_fusion), channel_id=1, replica_groups=mesh['sp_0'=8,'sp_1'=4,'fs'=4,'tp'=2] {'tp'}, dimensions={0} | all-to-all | bytes 262144 | tf_op jit(solution)/shard_map/all_to_all | solution.py:285
  404.6 3.9 all_to_all.42
  408.5 3.6 fusion.229
  412.1 4.3 %fusion.1 = bf16[1,64,2048]{2,1,0:T(8,128)(2,1)} fusion(f32[64,2048]{1,0:T(8,128)S(1)} %fusion.229, bf16[64,1024]{1,0:T(8,128)(2,1)S(1)} %bitcast.409, bf16[2048,1024]{1,0:T(8,128)(2,1)} %all-gather.28.cloned.1.call-done), kind=kOutput, calls=%fused_computation.2 | convolution fusion | flops 268697600 | bytes 5111808 | tf_op jit(solution)/shard_map/dot_general | solution.py:85
  (340 shorter events, 96.8 us)
Async XLA Ops:
  6.5 9.9 %copy-start = (bf16[2048,128]{1,0:T(8,128)(2,1)S(1)}, bf16[2048,128]{1,0:T(8,128)(2,1)}, u32[]{:S(2)}) copy-start(bf16[2048,128]{1,0:T(8,128)(2,1)} %param.24) | copy-start | bytes 1572868
  6.5 52.6 %all-gather.18.cloned.1.call-start = ((), (), s32[]{:S(2)}) async-start(), calls=%async_computation.4 | async-start | bytes 2621440 | tf_op jit(solution)/shard_map/all_gather | solution.py:157
  7.3 308.9 %all-gather.16.cloned.1.call-start = ((), (), s32[]{:S(2)}) async-start(), calls=%async_computation.3 | async-start | bytes 2621440 | tf_op jit(solution)/shard_map/all_gather | solution.py:156
  8.0 311.1 %all-gather.20.cloned.1.call-start = ((), (), s32[]{:S(2)}) async-start(), calls=%async_computation.5 | async-start | bytes 2621440 | tf_op jit(solution)/shard_map/all_gather | solution.py:160
  8.7 343.6 %all-gather.26.cloned.1.call-start = ((), (), s32[]{:S(2)}) async-start(), calls=%async_computation.8 | async-start | bytes 2621440 | tf_op jit(solution)/shard_map/all_gather | solution.py:161
  10.9 5.4 %copy-start.68 = (bf16[2048]{0:T(1024)(128)(2,1)S(1)}, bf16[2048]{0:T(1024)(128)(2,1)}, u32[]{:S(2)}) copy-start(bf16[2048]{0:T(1024)(128)(2,1)} %param.19) | copy-start | bytes 12292
  10.9 5.4 %copy-start.5 = (bf16[1,128,2048]{2,1,0:T(8,128)(2,1)S(1)}, bf16[1,128,2048]{2,1,0:T(8,128)(2,1)}, u32[]{:S(2)}) copy-start(bf16[1,128,2048]{2,1,0:T(8,128)(2,1)} %param.18) | copy-start | bytes 1572868
  10.9 42.7 %all-to-all-start = ((bf16[4,512,512]{2,1,0:T(8,128)(2,1)}), bf16[4,512,512]{2,1,0:T(8,128)(2,1)}, u32[]{:S(2)}, u32[]{:S(2)}) async-start(bf16[4,512,512]{2,1,0:T(8,128)(2,1)} %tile.2), calls=%async_computation | async-start | bytes 4194304 | tf_op jit(solution)/shard_map/all_to_all | solution.py:24
  15.5 337.5 %all-gather.24.cloned.1.call-start = ((), (), s32[]{:S(2)}) async-start(), calls=%async_computation.7 | async-start | bytes 2621440 | tf_op jit(solution)/shard_map/all_gather | solution.py:159
  16.1 392.3 %all-gather.22.cloned.1.call-start = ((), (), s32[]{:S(2)}) async-start(), calls=%async_computation.6 | async-start | bytes 6291456 | tf_op jit(solution)/shard_map/all_gather | solution.py:289
  16.5 42.7 %copy-start.63 = (f32[128]{0:T(128)}, f32[128]{0:T(128)S(1)}, u32[]{:S(2)}) copy-start(f32[128]{0:T(128)S(1)} %add_rsqrt_fusion.2) | copy-start | bytes 1540
  21.9 33.8 %copy-start.25 = (f32[1,4,32,8,64]{4,3,1,2,0:T(8,128)}, f32[1,4,32,8,64]{4,3,1,2,0:T(8,128)S(1)}, u32[]{:S(2)}) copy-start(f32[1,4,32,8,64]{4,3,1,2,0:T(8,128)S(1)} %fusion.77) | copy-start | bytes 786436
  57.1 33.8 %copy-start.19 = (f32[128,8,64]{2,0,1:T(8,128)}, f32[128,8,64]{2,0,1:T(8,128)S(1)}, u32[]{:S(2)}) copy-start(f32[128,8,64]{2,0,1:T(8,128)S(1)} %copy.128) | copy-start | bytes 786436
  58.5 32.4 %copy-start.22 = (f32[1,4,32,8,64]{4,2,1,3,0:T(8,128)}, f32[1,4,32,8,64]{4,2,1,3,0:T(8,128)S(1)}, u32[]{:S(2)}) copy-start(f32[1,4,32,8,64]{4,2,1,3,0:T(8,128)S(1)} %copy.129) | copy-start | bytes 786436
  73.2 11.7 %copy-start.7 = (f32[2,8,4,32,64]{4,1,2,3,0:T(8,128)}, f32[2,8,4,32,64]{4,1,2,3,0:T(8,128)S(1)}, u32[]{:S(2)}) copy-start(f32[2,8,4,32,64]{4,1,2,3,0:T(8,128)S(1)} %get-tuple-element.12) | copy-start | bytes 1572868
  90.9 6.6 %copy-start.11 = (f32[2,8,4,32,64]{4,3,2,1,0:T(8,128)}, f32[2,8,4,32,64]{4,3,2,1,0:T(8,128)S(1)}, u32[]{:S(2)}) copy-start(f32[2,8,4,32,64]{4,3,2,1,0:T(8,128)S(1)} %convolution_negate_fusion.1) | copy-start | bytes 1572868
  101.3 11.3 %copy-start.2 = (f32[2,8,4,64,64]{4,3,2,1,0:T(8,128)}, f32[2,8,4,64,64]{4,3,2,1,0:T(8,128)S(1)}, u32[]{:S(2)}) copy-start(f32[2,8,4,64,64]{4,3,2,1,0:T(8,128)S(1)} %multiply_add_fusion) | copy-start | bytes 3145732
  115.6 11.3 %slice-start.1 = ((f32[2,8,4,64,64]{4,3,2,1,0:T(8,128)}), f32[2,8,1,64,64]{4,3,2,1,0:T(8,128)S(1)}, s32[]{:S(2)}) async-start(f32[2,8,4,64,64]{4,3,2,1,0:T(8,128)} %copy-done.15), calls=%async_computation.11 | async-start | bytes 1048576 | tf_op jit(solution)/shard_map/slice | solution.py:219
  115.6 11.3 %copy-start.53 = (f32[2,8,1,64,64]{4,3,2,1,0:T(8,128)S(1)}, f32[2,8,1,64,64]{4,3,2,1,0:T(8,128)}, u32[]{:S(2)}) copy-start(f32[2,8,1,64,64]{4,3,2,1,0:T(8,128)} %fusion.15) | copy-start | bytes 786436
  127.0 11.2 %slice-start = ((f32[2,8,4,64,64]{4,3,2,1,0:T(8,128)}), f32[2,8,1,64,64]{4,3,2,1,0:T(8,128)S(1)}, s32[]{:S(2)}) async-start(f32[2,8,4,64,64]{4,3,2,1,0:T(8,128)} %copy-done.2), calls=%async_computation.10 | async-start | bytes 1048576 | tf_op jit(solution)/shard_map/slice | solution.py:219
  127.0 11.2 %copy-start.54 = (f32[2,8,1,64,64]{4,3,2,1,0:T(8,128)S(1)}, f32[2,8,1,64,64]{4,3,2,1,0:T(8,128)}, u32[]{:S(2)}) copy-start(f32[2,8,1,64,64]{4,3,2,1,0:T(8,128)} %convolution_bitcast_fusion.3) | copy-start | bytes 786436
  149.6 16.7 %copy-start.3 = (f32[2,8,4,64,64]{4,3,2,1,0:T(8,128)S(1)}, f32[2,8,4,64,64]{4,3,2,1,0:T(8,128)}, u32[]{:S(2)}) copy-start(f32[2,8,4,64,64]{4,3,2,1,0:T(8,128)} %pad.33) | copy-start | bytes 3145732
  166.3 12.1 %copy-start.17 = (f32[2,8,4,64,64]{4,3,2,1,0:T(8,128)S(1)}, f32[2,8,4,64,64]{4,3,2,1,0:T(8,128)}, u32[]{:S(2)}) copy-start(f32[2,8,4,64,64]{4,3,2,1,0:T(8,128)} %pad.28) | copy-start | bytes 3145732
  166.3 12.1 %copy-start.18 = (f32[2,8,4,64,64]{4,3,2,1,0:T(8,128)S(1)}, f32[2,8,4,64,64]{4,3,2,1,0:T(8,128)}, u32[]{:S(2)}) copy-start(f32[2,8,4,64,64]{4,3,2,1,0:T(8,128)} %pad.29) | copy-start | bytes 3145732
  192.9 28.4 %copy-start.32 = (f32[8,64,64]{2,1,0:T(8,128)}, f32[8,64,64]{2,1,0:T(8,128)S(1)}, u32[]{:S(2)}) copy-start(f32[8,64,64]{2,1,0:T(8,128)S(1)} %convolution_add_fusion.19) | copy-start | bytes 393220
  193.2 28.4 %copy-start.33 = (f32[8,64,64]{2,1,0:T(8,128)}, f32[8,64,64]{2,1,0:T(8,128)S(1)}, u32[]{:S(2)}) copy-start(f32[8,64,64]{2,1,0:T(8,128)S(1)} %convolution_add_fusion.18) | copy-start | bytes 393220
  265.3 22.4 %copy-start.44 = (f32[8,64,64]{2,1,0:T(8,128)}, f32[8,64,64]{2,1,0:T(8,128)S(1)}, u32[]{:S(2)}) copy-start(f32[8,64,64]{2,1,0:T(8,128)S(1)} %convolution_add_fusion.33) | copy-start | bytes 393220
  287.5 24.8 %copy-start.27 = (bf16[64,64,64]{2,1,0:T(8,128)(2,1)}, bf16[64,64,64]{2,1,0:T(8,128)(2,1)S(1)}, u32[]{:S(2)}) copy-start(bf16[64,64,64]{2,1,0:T(8,128)(2,1)S(1)} %all-gather.3) | copy-start | bytes 1572868
  319.2 92.9 %all-gather.28.cloned.1.call-start = ((), (), s32[]{:S(2)}) async-start(), calls=%async_computation.9 | async-start | bytes 6291456 | tf_op jit(solution)/shard_map/all_gather | solution.py:290
  352.8 10.1 %copy-start.65 = (f32[512]{0:T(512)S(1)}, f32[512]{0:T(512)}, u32[]{:S(2)}) copy-start(f32[512]{0:T(512)} %convert_element_type.442) | copy-start | bytes 6148
  355.5 47.3 %collective-permute-start.1 = (bf16[8,512]{1,0:T(8,128)(2,1)S(1)}, bf16[8,512]{1,0:T(8,128)(2,1)S(1)}, u32[]{:S(2)}, u32[]{:S(2)}) collective-permute-start(bf16[8,512]{1,0:T(8,128)(2,1)S(1)} %get-tuple-element.35), channel_id=1, source_target_pairs={{8,0},{16,8},{24,16},{32,24},{40,32},{48,40},{56,48},{64,56},{72,6... | collective-permute-start | bytes 24584 | tf_op jit(solution)/shard_map/ppermute | solution.py:65
  357.4 45.4 %collective-permute-start = (bf16[8,512]{1,0:T(8,128)(2,1)S(1)}, bf16[8,512]{1,0:T(8,128)(2,1)S(1)}, u32[]{:S(2)}, u32[]{:S(2)}) collective-permute-start(bf16[8,512]{1,0:T(8,128)(2,1)S(1)} %get-tuple-element.34), channel_id=1, source_target_pairs={{0,8},{8,16},{16,24},{24,32},{32,40},{40,48},{48,56},{56,64},{64,7... | collective-permute-start | bytes 24584 | tf_op jit(solution)/shard_map/ppermute | solution.py:63
  (57 other events, 127.6 us)
Sparse Core Ops, SparseCore 0:
  9.1 49.9 all-gather.17
  61.0 34.2 all-gather.15
  97.1 33.3 all-gather.19
  132.1 33.3 all-gather.25
  167.2 33.3 all-gather.23
  319.3 51.1 all-gather.21
  372.3 31.7 all-gather.27
